TPU v7x, 32 devices: a whole 2x2x4 slice. The times are simulated.
32 devices in a mesh: sp: 4 (over y, core), tp: 8 (over z, x).
Axes of the slice: x: 2, y: 2, z: 4, core: 2. Of those that a mesh axis runs over, the one named last changes fastest.
Arguments:
- latent: bfloat16 [960, 2048], P(('sp', 'tp')), may hold values from -40 to 40
- context: bfloat16 [768, 2048], P('sp'), may hold values from -6 to 6
- cond_latent: float32 [2048], P('sp'), may hold values from -6 to 6
- cond_context: float32 [2048], P('sp'), may hold values from -6 to 6
- mod_weight: bfloat16 [2048, 6144], P('sp', 'tp'), may hold values from -0.125 to 0.125
- w_query: bfloat16 [2048, 1024], P(None, 'tp'), may hold values from -5 to 5
- w_key: bfloat16 [2048, 1024], P(None, 'tp'), may hold values from -5 to 5
- w_value: bfloat16 [2048, 1024], P(None, 'tp'), may hold values from -0.125 to 0.125
- w_out: bfloat16 [1024, 2048], P('tp'), may hold values from -0.1875 to 0.1875
- head_lambda: float32 [8], P('tp'), may hold values from 0.3 to 0.8
Outputs:
- mixed_latent: bfloat16 [960, 2048], P(('sp', 'tp'))
All inputs are finite; a program needn't handle non-finite values.
Results may differ from a plain program's by a relative error of at most 0.011.
Values may be sent and summed in bfloat16 or wider, within the bound.
A program may use at most 64 MiB of HBM per device.

v0:
```python
import jax
import jax.numpy as jnp
from jax import lax
from jax.sharding import PartitionSpec as P

QK_DIM = 64
VAL_DIM = 128
GRID_W = 64
NORM_EPS = 0.01
HEAD_EPS = 0.001
THETA = 10000.0


def modulate_rows(rows, shift, scale):
    values = rows.astype(jnp.float32)
    normed = values * lax.rsqrt(jnp.mean(values * values, axis=-1, keepdims=True) + NORM_EPS)
    return (normed * (1.0 + scale) + shift).astype(jnp.bfloat16)


def rotary_tables(positions):
    quarter = QK_DIM // 4
    inverse = THETA ** (-jnp.arange(quarter, dtype=jnp.float32) / quarter)
    grid_row = (positions // GRID_W).astype(jnp.float32)
    grid_column = (positions % GRID_W).astype(jnp.float32)
    by_row = grid_row[:, None] * inverse[None, :]
    by_column = grid_column[:, None] * inverse[None, :]
    angle = jnp.concatenate([by_row, by_row, by_column, by_column], axis=-1)
    return (jnp.cos(angle), jnp.sin(angle))


def rotate(product, cosine, sine):
    number = product.shape[0]
    quarter = QK_DIM // 4
    half = QK_DIM // 2
    shaped = product.reshape(number, -1, QK_DIM)
    first = shaped[..., :half]
    second = shaped[..., half:]
    turned = jnp.concatenate(
        [
            -first[..., quarter:],
            first[..., :quarter],
            -second[..., quarter:],
            second[..., :quarter],
        ],
        axis=-1,
    )
    result = shaped * cosine[:, None, :] + turned * sine[:, None, :]
    return result.reshape(number, -1).astype(jnp.bfloat16)


def attend_piece(state, piece, queries):
    highest, totals, carried = state
    keys, values = piece
    number = keys.shape[0]
    heads = queries.shape[1]
    key_heads = keys.reshape(number, heads, 2, QK_DIM)
    value_heads = values.reshape(number, heads, VAL_DIM)
    scores = jnp.einsum(
        "qhmd,khmd->hmqk", queries, key_heads, preferred_element_type=jnp.float32
    ) * QK_DIM ** (-0.5)
    new_highest = jnp.maximum(highest, jnp.max(scores, axis=-1))
    weights = jnp.exp(scores - new_highest[..., None])
    totals = jnp.sum(weights, axis=-1)
    mixed = jnp.einsum(
        "hmqk,khd->hmqd",
        weights.astype(jnp.bfloat16),
        value_heads,
        preferred_element_type=jnp.float32,
    )
    carried = mixed
    return (new_highest, totals, carried)


def shards(
    latent,
    context,
    cond_latent,
    cond_context,
    mod_weight,
    w_query,
    w_key,
    w_value,
    w_out,
    head_lambda,
):
    width = latent.shape[1]
    heads = head_lambda.shape[0]
    conditioned = jax.nn.silu(jnp.stack([cond_latent, cond_context])).astype(jnp.bfloat16)
    partial_mod = jnp.dot(conditioned, mod_weight, preferred_element_type=jnp.float32)
    summed = lax.psum(partial_mod, "sp")
    modulation = lax.all_gather(summed, "tp", axis=1, tiled=True)
    shift_context = modulation[1, :width]
    scale_context = modulation[1, width : 2 * width]
    gate_latent = modulation[0, 2 * width :]
    own_rows = modulate_rows(latent, modulation[0, :width], modulation[0, width : 2 * width])
    group_rows = latent.shape[0] * lax.axis_size("tp")
    offset = lax.axis_index("sp") * group_rows
    piece = lax.all_gather(own_rows, "tp", axis=0, tiled=True)
    positions = offset + jnp.arange(piece.shape[0], dtype=jnp.int32)
    cosine, sine = rotary_tables(positions)
    query_part = rotate(jnp.dot(piece, w_query, preferred_element_type=jnp.float32), cosine, sine)
    key_part = rotate(jnp.dot(piece, w_key, preferred_element_type=jnp.float32), cosine, sine)
    value_part = jnp.dot(piece, w_value, preferred_element_type=jnp.float32).astype(jnp.bfloat16)
    projected = jnp.concatenate([query_part, key_part, value_part], axis=1)
    key_columns = heads * 2 * QK_DIM
    queries = projected[:, :key_columns].reshape(group_rows, heads, 2, QK_DIM)
    keys = projected[:, key_columns : 2 * key_columns]
    values = projected[:, 2 * key_columns :]
    initial = (
        jnp.full((heads, 2, group_rows), -1e30, jnp.float32),
        jnp.zeros((heads, 2, group_rows), jnp.float32),
        jnp.zeros((heads, 2, group_rows, VAL_DIM), jnp.float32),
    )
    own_context = modulate_rows(context, shift_context, scale_context)
    context_keys = jnp.dot(own_context, w_key, preferred_element_type=jnp.float32).astype(
        jnp.bfloat16
    )
    context_values = jnp.dot(own_context, w_value, preferred_element_type=jnp.float32).astype(
        jnp.bfloat16
    )
    joined_keys = jnp.concatenate([keys, context_keys], axis=0)
    joined_values = jnp.concatenate([values, context_values], axis=0)
    state = attend_piece(
        initial,
        (
            lax.all_gather(joined_keys, "sp", axis=0, tiled=True),
            lax.all_gather(joined_values, "sp", axis=0, tiled=True),
        ),
        queries,
    )
    highest, totals, carried = state
    factor = head_lambda[:, None, None]
    head_out = (
        carried[:, 0] / totals[:, 0][..., None] - factor * carried[:, 1] / totals[:, 1][..., None]
    )
    head_out = head_out * lax.rsqrt(
        jnp.mean(head_out * head_out, axis=-1, keepdims=True) + HEAD_EPS
    )
    attended = (
        jnp.transpose(head_out, (1, 0, 2)).reshape(group_rows, heads * VAL_DIM).astype(jnp.bfloat16)
    )
    branch = lax.psum_scatter(
        jnp.dot(attended, w_out, preferred_element_type=jnp.float32),
        "tp",
        scatter_dimension=0,
        tiled=True,
    )
    branch = branch * lax.rsqrt(jnp.mean(branch * branch, axis=-1, keepdims=True) + NORM_EPS)
    return (latent.astype(jnp.float32) + gate_latent * branch).astype(jnp.bfloat16)


def solution(mesh):
    placed = (
        P(("sp", "tp"), None),
        P("sp", None),
        P("sp"),
        P("sp"),
        P("sp", "tp"),
        P(None, "tp"),
        P(None, "tp"),
        P(None, "tp"),
        P("tp", None),
        P("tp"),
    )
    return jax.shard_map(
        shards, mesh=mesh, in_specs=placed, out_specs=P(("sp", "tp"), None), check_vma=False
    )
```

profile of v0, /device:TPU:8, one launch (start us, length us, event | category | flops | bytes accessed | tf_op | source)
XLA Modules:
  0.0 153.3 jit_solution(12564381263375404381)
XLA Ops:
  0.0 0.0 copy-start
  0.0 1.1 fusion.14
  1.1 0.0 copy-start.2
  1.2 0.0 copy-start.3
  1.2 1.5 fusion.6
  2.6 0.0 copy-done
  2.7 0.9 fusion.37
  3.6 7.0 %psum.7 = f32[2,768]{1,0:T(2,128)S(1)} all-reduce(f32[2,768]{1,0:T(2,128)S(1)} %fusion.37), channel_id=1, replica_groups=mesh['sp'=4,'tp'=8] {'sp'}, use_global_device_ids=true, to_apply=%region_0.1 | all-reduce | flops 1536 | bytes 12288 | tf_op jit(solution)/shard_map/psum | solution.py:90
  10.6 28.2 %all_gather.12 = f32[2,6144]{1,0:T(2,128)S(1)} all-gather(f32[2,768]{1,0:T(2,128)S(1)} %psum.7), channel_id=1, replica_groups=mesh['sp'=4,'tp'=8] {'tp'}, dimensions={1}, use_global_device_ids=true | all-gather | bytes 55296 | tf_op jit(solution)/shard_map/all_gather | solution.py:91
  38.9 0.0 copy-start.1
  38.9 1.8 %convolution_convert_fusion.1 = bf16[192,128]{1,0:T(8,128)(2,1)S(1)} fusion(bf16[2048,128]{1,0:T(8,128)(2,1)} %param.17, bf16[192,2048]{1,0:T(8,128)(2,1)} %param.11, f32[2048]{0:T(1024)S(1)} %bitcast.84, f32[2048]{0:T(1024)S(1)} %bitcast.86, f32[192]{0:T(256)S(1)} %add_rsqrt_fusion.1), kind=kOutput, calls=%fused_computation.14 | convolution fusion | flops 102653952 | bytes 1377024 | tf_op jit(solution)/shard_map/dot_general | solution.py:118
  40.7 0.0 copy-done.2
  40.7 0.0 copy-done.3
  40.7 0.5 convolution_convert_fusion.2
  41.2 0.0 copy-done.1
  41.2 0.1 fusion.19
  41.3 33.0 %all-gather = bf16[8,30,2048]{2,1,0:T(8,128)(2,1)S(1)} all-gather(bf16[1,30,2048]{2,1,0:T(8,128)(2,1)S(1)} %fusion.19), channel_id=1, replica_groups=mesh['sp'=4,'tp'=8] {'tp'}, dimensions={0}, use_global_device_ids=true | all-gather | bytes 1105920 | tf_op jit(solution)/shard_map/all_gather | solution.py:98
  74.3 0.3 reshape.355
  74.6 0.0 copy-start.4
  74.6 1.5 convolution_convert_fusion
  76.1 1.4 fusion.49
  78.2 0.1 broadcast_multiply_fusion.1
  78.3 0.1 fusion.35
  78.4 0.1 copy.21
  78.5 0.0 copy-done.4
  78.5 0.4 fusion.48
  78.9 0.1 copy.22
  79.0 0.1 copy.26
  79.2 0.1 copy.27
  79.3 0.1 copy.23
  79.5 0.1 copy.24
  79.6 6.3 %all_gather.14 = bf16[1728,128]{1,0:T(8,128)(2,1)S(1)} all-gather(bf16[432,128]{1,0:T(8,128)(2,1)S(1)} %pad_maximum_fusion), channel_id=1, replica_groups=mesh['sp'=4,'tp'=8] {'sp'}, dimensions={0}, use_global_device_ids=true | all-gather | bytes 552960 | tf_op jit(solution)/shard_map/all_gather | solution.py:126
  85.9 0.2 copy.28
  86.1 6.8 %all_gather.15 = bf16[1728,128]{1,0:T(8,128)(2,1)S(1)} all-gather(bf16[432,128]{1,0:T(8,128)(2,1)S(1)} %pad_maximum_fusion.1), channel_id=1, replica_groups=mesh['sp'=4,'tp'=8] {'sp'}, dimensions={0}, use_global_device_ids=true | all-gather | bytes 552960 | tf_op jit(solution)/shard_map/all_gather | solution.py:127
  92.9 0.7 fusion.47
  93.7 0.6 fusion.1
  94.3 0.0 copy-start.5
  94.3 0.7 fusion.10
  95.0 0.2 fusion.27
  95.2 0.1 copy-done.5
  95.3 0.0 copy-start.6
  95.3 0.5 fusion.28
  95.8 48.5 %fusion = f32[32,2048]{1,0:T(8,128)S(1)} fusion(f32[240,2048]{1,0:T(8,128)S(1)} %fusion.28), kind=kCustom, calls=%all-reduce-scatter | all-reduce-scatter fusion | flops 524289 | bytes 2228736
  144.3 4.3 %collective-permute-start = (f32[14,2048]{1,0:T(8,128)S(1)}, f32[14,2048]{1,0:T(8,128)S(1)}, u32[]{:S(2)}, u32[]{:S(2)}) collective-permute-start(f32[14,2048]{1,0:T(8,128)S(1)} %slice.97), channel_id=1, source_target_pairs={{0,1},{1,2},{2,3},{3,4},{4,5},{5,6},{6,7},{8,9},{9,10},{10,11},{11... | collective-permute-start | bytes 344072
  148.6 0.0 copy-done.6
  148.6 0.6 dynamic-slice.4
  149.9 2.2 %collective-permute-done = f32[14,2048]{1,0:T(8,128)S(1)} collective-permute-done((f32[14,2048]{1,0:T(8,128)S(1)}, f32[14,2048]{1,0:T(8,128)S(1)}, u32[]{:S(2)}, u32[]{:S(2)}) %collective-permute-start) | collective-permute-done | bytes 114720
  152.1 0.2 concatenate.28
  152.4 0.2 multiply_reduce_fusion
  152.5 0.8 fusion.18
  (16 shorter events, 0.2 us)
Async XLA Ops:
  0.0 2.6 %copy-start = (bf16[512,768]{1,0:T(8,128)(2,1)S(1)}, bf16[512,768]{1,0:T(8,128)(2,1)}, u32[]{:S(2)}) copy-start(bf16[512,768]{1,0:T(8,128)(2,1)} %param.14) | copy-start | bytes 2359300
  1.1 39.6 %copy-start.2 = (bf16[192,2048]{1,0:T(8,128)(2,1)S(1)}, bf16[192,2048]{1,0:T(8,128)(2,1)}, u32[]{:S(2)}) copy-start(bf16[192,2048]{1,0:T(8,128)(2,1)} %param.11) | copy-start | bytes 2359300
  1.2 39.5 %copy-start.3 = (bf16[2048,128]{1,0:T(8,128)(2,1)S(1)}, bf16[2048,128]{1,0:T(8,128)(2,1)}, u32[]{:S(2)}) copy-start(bf16[2048,128]{1,0:T(8,128)(2,1)} %param.16) | copy-start | bytes 1572868
  38.9 2.3 %copy-start.1 = (bf16[30,2048]{1,0:T(8,128)(2,1)S(1)}, bf16[30,2048]{1,0:T(8,128)(2,1)}, u32[]{:S(2)}) copy-start(bf16[30,2048]{1,0:T(8,128)(2,1)} %param.10) | copy-start | bytes 368644
  74.6 4.0 %copy-start.4 = (bf16[2048,128]{1,0:T(8,128)(2,1)S(1)}, bf16[2048,128]{1,0:T(8,128)(2,1)}, u32[]{:S(2)}) copy-start(bf16[2048,128]{1,0:T(8,128)(2,1)} %param.15) | copy-start | bytes 1572868
  94.3 1.0 copy-start.5
  95.3 53.3 %copy-start.6 = (u32[32]{0:T(128)S(1)}, u32[32]{0:T(128)}, u32[]{:S(2)}) copy-start(u32[32]{0:T(128)} %constant.70) | copy-start | bytes 388
  144.3 7.8 %collective-permute-start = (f32[14,2048]{1,0:T(8,128)S(1)}, f32[14,2048]{1,0:T(8,128)S(1)}, u32[]{:S(2)}, u32[]{:S(2)}) collective-permute-start(f32[14,2048]{1,0:T(8,128)S(1)} %slice.97), channel_id=1, source_target_pairs={{0,1},{1,2},{2,3},{3,4},{4,5},{5,6},{6,7},{8,9},{9,10},{10,11},{11... | collective-permute-start | bytes 344072
where the time goes:
time: 154 us; the launch traced here: 153 us
  blocking collectives  130 us (84%)
  matrix products  8.4 us (5%)
  other arithmetic  4.88 us (3%)
  starting transfers between devices  4.27 us (3%)
  waiting for transfers between devices  2.24 us (1%)
  local copies, waits for them, and re-layouts  2.05 us (1%)
  between operations  1.61 us (1%)
    unnamed x1, blocking collectives  48.5 us
    all_gather x1, blocking collectives, shards(): piece = lax.all_gather(own_rows, 'tp', axis=0, tiled=True)  33 us
    all_gather x1, blocking collectives, shards(): modulation = lax.all_gather(summed, 'tp', axis=1, tiled=True)  28.2 us
    psum x1, blocking collectives, shards(): summed = lax.psum(partial_mod, 'sp')  7.04 us
    all_gather x1, blocking collectives, shards(): lax.all_gather(joined_values, 'sp', axis=0, tiled=True)  6.83 us
    all_gather x1, blocking collectives, shards(): lax.all_gather(joined_keys, 'sp', axis=0, tiled=True)  6.28 us
    unnamed x1, starting transfers between devices  4.27 us
  transfers between devices with their start and end apart: 1, of which 1 were waited for; matrix products, arithmetic and copies ran while one was open for 0% of the time, Pallas kernels for 0%

commit v1 on v0

--- a/solution.py
+++ b/solution.py
@@ -88,7 +88,9 @@
     conditioned = jax.nn.silu(jnp.stack([cond_latent, cond_context])).astype(jnp.bfloat16)
     partial_mod = jnp.dot(conditioned, mod_weight, preferred_element_type=jnp.float32)
     summed = lax.psum(partial_mod, "sp")
-    modulation = lax.all_gather(summed, "tp", axis=1, tiled=True)
+    modulation = jnp.concatenate(
+        lax.all_to_all(jnp.stack([summed] * lax.axis_size("tp")), "tp", 0, 0), axis=1
+    )
     shift_context = modulation[1, :width]
     scale_context = modulation[1, width : 2 * width]
     gate_latent = modulation[0, 2 * width :]

time: 154 us -> 132 us (0.86)
  blocking collectives: 130 us -> 99.6 us
  starting transfers between devices: 4.27 us -> 8.17 us
  waiting for transfers between devices: 2.24 us -> 6.14 us
  local copies, waits for them, and re-layouts: 2.05 us -> 3.8 us
    all_gather x1 -> x0, blocking collectives: 28.2 us -> none  [shards(): modulation = lax.all_gather(summed, 'tp', axis=1, tiled=True)]
    all_to_all x0 -> x1, starting transfers between devices: none -> 6.25 us  [shards(): lax.all_to_all(jnp.stack([summed] * lax.axis_size('tp')), 'tp', 0, 0)]
    unnamed x1, starting transfers between devices: 4.27 us -> 1.92 us
    unnamed x1, waiting for transfers between devices: 2.24 us -> 4.58 us
    all_gather x1, blocking collectives: 33 us -> 31.1 us  [shards(): piece = lax.all_gather(own_rows, 'tp', axis=0, tiled=True)]
    all_to_all x0 -> x1, waiting for transfers between devices: none -> 1.55 us  [shards(): lax.all_to_all(jnp.stack([summed] * lax.axis_size('tp')), 'tp', 0, 0)]
  transfers between devices with their start and end apart: 1 -> 2, of which waited for: 1 -> 2; matrix products, arithmetic and copies ran while one was open for 0% -> 3% of each run, Pallas kernels for 0% -> 0%
where the time goes in v1:
time: 132 us; the launch traced here: 131 us
  blocking collectives  99.6 us (75%)
  starting transfers between devices  8.17 us (6%)
  matrix products  7.1 us (5%)
  waiting for transfers between devices  6.14 us (5%)
  other arithmetic  4.77 us (4%)
  local copies, waits for them, and re-layouts  3.8 us (3%)
  between operations  1.62 us (1%)
    unnamed x1, blocking collectives  48.4 us
    all_gather x1, blocking collectives, shards(): piece = lax.all_gather(own_rows, 'tp', axis=0, tiled=True)  31.1 us
    psum x1, blocking collectives, shards(): summed = lax.psum(partial_mod, 'sp')  7.04 us
    all_gather x1, blocking collectives, shards(): lax.all_gather(joined_values, 'sp', axis=0, tiled=True)  6.83 us
    all_gather x1, blocking collectives, shards(): lax.all_gather(joined_keys, 'sp', axis=0, tiled=True)  6.28 us
    all_to_all x1, starting transfers between devices, shards(): lax.all_to_all(jnp.stack([summed] * lax.axis_size('tp')), 'tp', 0, 0)  6.25 us
    unnamed x1, waiting for transfers between devices  4.58 us
  transfers between devices with their start and end apart: 2, of which 2 were waited for; matrix products, arithmetic and copies ran while one was open for 3% of the time, Pallas kernels for 0%

profile of v1, /device:TPU:8, one launch (start us, length us, event | category | flops | bytes accessed | tf_op | source)
XLA Modules:
  0.0 131.2 jit_solution(12008951585253511056)
XLA Ops:
  0.0 0.0 copy-start
  0.0 0.0 copy-start.2
  0.0 0.0 copy-start.3
  0.0 1.1 copy-done
  1.1 0.9 fusion.37
  2.0 7.0 %psum.7 = f32[2,768]{1,0:T(2,128)S(1)} all-reduce(f32[2,768]{1,0:T(2,128)S(1)} %fusion.37), channel_id=1, replica_groups=mesh['sp'=4,'tp'=8] {'sp'}, use_global_device_ids=true, to_apply=%region_0.1 | all-reduce | flops 1536 | bytes 12288 | tf_op jit(solution)/shard_map/psum | solution.py:90
  9.1 0.6 stack.11
  9.7 6.3 %all-to-all-start = ((f32[8,2,768]{2,1,0:T(2,128)}), f32[8,2,768]{2,1,0:T(2,128)S(1)}, u32[]{:S(2)}, u32[]{:S(2)}) async-start(f32[8,2,768]{2,1,0:T(2,128)} %stack.11), calls=%async_computation | async-start | bytes 98304 | tf_op jit(solution)/shard_map/all_to_all | solution.py:92
  16.6 0.0 copy-start.4
  16.7 1.1 fusion.14
  17.8 1.4 %fusion.6 = f32[192]{0:T(256)S(1)} fusion(bf16[192,2048]{1,0:T(8,128)(2,1)} %param.11), kind=kLoop, calls=%fused_computation.8 | loop fusion | flops 1179456 | bytes 787200 | tf_op jit(solution)/shard_map/reduce_sum | solution.py:16
  19.2 0.1 broadcast_multiply_fusion.1
  19.3 0.1 fusion.35
  19.4 0.1 copy.21
  19.5 1.6 %all-to-all-done = f32[8,2,768]{2,1,0:T(2,128)S(1)} async-done(((f32[8,2,768]{2,1,0:T(2,128)}), f32[8,2,768]{2,1,0:T(2,128)S(1)}, u32[]{:S(2)}, u32[]{:S(2)}) %all-to-all-start) | async-done | bytes 49184 | tf_op jit(solution)/shard_map/all_to_all | solution.py:92
  21.1 0.0 copy-done.2
  21.1 0.0 copy-done.3
  21.1 0.0 copy-start.1
  21.1 0.5 convolution_convert_fusion.1
  21.6 0.0 copy-done.4
  21.6 0.5 convolution_convert_fusion.2
  22.1 0.0 copy-done.1
  22.1 0.1 fusion.19
  22.2 31.1 %all-gather = bf16[8,30,2048]{2,1,0:T(8,128)(2,1)S(1)} all-gather(bf16[1,30,2048]{2,1,0:T(8,128)(2,1)S(1)} %fusion.19), channel_id=1, replica_groups=mesh['sp'=4,'tp'=8] {'tp'}, dimensions={0}, use_global_device_ids=true | all-gather | bytes 1105920 | tf_op jit(solution)/shard_map/all_gather | solution.py:100
  53.3 0.3 reshape.365
  53.5 0.0 copy-start.5
  53.6 1.5 %convolution_convert_fusion = bf16[240,128]{1,0:T(8,128)(2,1)S(1)} fusion(bf16[240,2048]{1,0:T(8,128)(2,1)S(1)} %reshape.365, bf16[2048,128]{1,0:T(8,128)(2,1)} %param.17), kind=kOutput, calls=%fused_computation.13 | convolution fusion | flops 125859840 | bytes 1568768 | tf_op jit(solution)/shard_map/dot_general | solution.py:105
  55.1 1.4 %fusion.49 = f32[240,128]{1,0:T(8,128)S(1)} fusion(bf16[240,2048]{1,0:T(8,128)(2,1)S(1)} %reshape.365, bf16[2048,128]{1,0:T(8,128)(2,1)} %param.16), kind=kOutput, calls=%fused_computation.87 | convolution fusion | flops 125829120 | bytes 1630208 | tf_op jit(solution)/shard_map/dot_general | solution.py:104
  56.5 0.0 copy-done.5
  56.5 0.4 fusion.48
  57.0 0.1 copy.22
  57.1 0.1 copy.26
  57.2 0.1 copy.27
  57.3 0.1 copy.23
  57.5 0.1 copy.24
  57.6 6.3 %all_gather.10 = bf16[1728,128]{1,0:T(8,128)(2,1)S(1)} all-gather(bf16[432,128]{1,0:T(8,128)(2,1)S(1)} %pad_maximum_fusion), channel_id=1, replica_groups=mesh['sp'=4,'tp'=8] {'sp'}, dimensions={0}, use_global_device_ids=true | all-gather | bytes 552960 | tf_op jit(solution)/shard_map/all_gather | solution.py:128
  63.9 0.2 copy.28
  64.1 6.8 %all_gather.11 = bf16[1728,128]{1,0:T(8,128)(2,1)S(1)} all-gather(bf16[432,128]{1,0:T(8,128)(2,1)S(1)} %pad_maximum_fusion.1), channel_id=1, replica_groups=mesh['sp'=4,'tp'=8] {'sp'}, dimensions={0}, use_global_device_ids=true | all-gather | bytes 552960 | tf_op jit(solution)/shard_map/all_gather | solution.py:129
  71.0 0.7 fusion.47
  71.7 0.6 fusion.1
  72.3 0.0 copy-start.6
  72.3 0.7 fusion.10
  73.0 0.2 fusion.27
  73.2 0.1 copy-done.6
  73.4 0.0 copy-start.7
  73.4 0.5 fusion.28
  73.9 48.4 %fusion = f32[32,2048]{1,0:T(8,128)S(1)} fusion(f32[240,2048]{1,0:T(8,128)S(1)} %fusion.28), kind=kCustom, calls=%all-reduce-scatter | all-reduce-scatter fusion | flops 524289 | bytes 2228736
  122.3 1.9 %collective-permute-start = (f32[14,2048]{1,0:T(8,128)S(1)}, f32[14,2048]{1,0:T(8,128)S(1)}, u32[]{:S(2)}, u32[]{:S(2)}) collective-permute-start(f32[14,2048]{1,0:T(8,128)S(1)} %slice.97), channel_id=1, source_target_pairs={{0,1},{1,2},{2,3},{3,4},{4,5},{5,6},{6,7},{8,9},{9,10},{10,11},{11... | collective-permute-start | bytes 344072
  124.2 0.0 copy-done.7
  124.2 0.6 dynamic-slice.4
  125.4 4.6 %collective-permute-done = f32[14,2048]{1,0:T(8,128)S(1)} collective-permute-done((f32[14,2048]{1,0:T(8,128)S(1)}, f32[14,2048]{1,0:T(8,128)S(1)}, u32[]{:S(2)}, u32[]{:S(2)}) %collective-permute-start) | collective-permute-done | bytes 114720
  130.0 0.2 concatenate.28
  130.3 0.2 multiply_reduce_fusion
  130.4 0.8 fusion.18
  (16 shorter events, 0.2 us)
Async XLA Ops:
  0.0 1.1 copy-start
  0.0 21.1 %copy-start.2 = (bf16[192,2048]{1,0:T(8,128)(2,1)S(1)}, bf16[192,2048]{1,0:T(8,128)(2,1)}, u32[]{:S(2)}) copy-start(bf16[192,2048]{1,0:T(8,128)(2,1)} %param.11) | copy-start | bytes 2359300
  0.0 21.1 %copy-start.3 = (bf16[2048,128]{1,0:T(8,128)(2,1)S(1)}, bf16[2048,128]{1,0:T(8,128)(2,1)}, u32[]{:S(2)}) copy-start(bf16[2048,128]{1,0:T(8,128)(2,1)} %param.17) | copy-start | bytes 1572868
  9.7 11.3 %all-to-all-start = ((f32[8,2,768]{2,1,0:T(2,128)}), f32[8,2,768]{2,1,0:T(2,128)S(1)}, u32[]{:S(2)}, u32[]{:S(2)}) async-start(f32[8,2,768]{2,1,0:T(2,128)} %stack.11), calls=%async_computation | async-start | bytes 98304 | tf_op jit(solution)/shard_map/all_to_all | solution.py:92
  16.6 4.9 %copy-start.4 = (bf16[2048,128]{1,0:T(8,128)(2,1)S(1)}, bf16[2048,128]{1,0:T(8,128)(2,1)}, u32[]{:S(2)}) copy-start(bf16[2048,128]{1,0:T(8,128)(2,1)} %param.16) | copy-start | bytes 1572868
  21.1 1.0 copy-start.1
  53.5 3.0 %copy-start.5 = (bf16[2048,128]{1,0:T(8,128)(2,1)S(1)}, bf16[2048,128]{1,0:T(8,128)(2,1)}, u32[]{:S(2)}) copy-start(bf16[2048,128]{1,0:T(8,128)(2,1)} %param.15) | copy-start | bytes 1572868
  72.3 1.0 copy-start.6
  73.4 50.8 %copy-start.7 = (u32[32]{0:T(128)S(1)}, u32[32]{0:T(128)}, u32[]{:S(2)}) copy-start(u32[32]{0:T(128)} %constant.70) | copy-start | bytes 388
  122.3 7.8 %collective-permute-start = (f32[14,2048]{1,0:T(8,128)S(1)}, f32[14,2048]{1,0:T(8,128)S(1)}, u32[]{:S(2)}, u32[]{:S(2)}) collective-permute-start(f32[14,2048]{1,0:T(8,128)S(1)} %slice.97), channel_id=1, source_target_pairs={{0,1},{1,2},{2,3},{3,4},{4,5},{5,6},{6,7},{8,9},{9,10},{10,11},{11... | collective-permute-start | bytes 344072
